TPU v7x, 32 devices: a whole 2x2x4 slice. The times are simulated.
32 devices in a mesh: ep: 16 (over z, y, x), tp: 2 (over core).
Axes of the slice: x: 2, y: 2, z: 4, core: 2. Of those that a mesh axis runs over, the one named last changes fastest.
Arguments:
- tokens: bfloat16 [256, 1024], P('ep'), may hold values from -6 to 6
- mixer_gain: float32 [1024], replicated, may hold values from 0.1 to 1.9
- query_weight: bfloat16 [1024, 1024], P(None, 'tp'), may hold values from -0.1875 to 0.1875
- key_weight: bfloat16 [1024, 256], P(None, 'tp'), may hold values from -0.1875 to 0.1875
- value_weight: bfloat16 [1024, 256], P(None, 'tp'), may hold values from -0.1875 to 0.1875
- head_lambda: float32 [8], P('tp'), may hold values from 0.3 to 0.8
- head_gain: float32 [128], replicated, may hold values from 0.1 to 1.9
- out_weight: bfloat16 [1024, 1024], P('tp'), may hold values from -0.1875 to 0.1875
- cache_keys: bfloat16 [256, 1024, 256], P('ep', None, 'tp'), may hold values from -700 to 700
- cache_values: bfloat16 [256, 1024, 256], P('ep', None, 'tp'), may hold values from -6 to 6
- seq_lengths: int32 [256], P('ep'), may hold values from 2 to 1024, as said below
- channel_gain: float32 [1024], replicated, may hold values from 0.1 to 1.9
- expert_ids: int32 [256, 6], P('ep'), may hold values from 0 to 15, all different within a row; in each aligned block of 16 rows (0 to 15, 16 to 31, ...) at most 12 rows name the same one
- expert_shares: bfloat16 [256, 6], P('ep'), may hold values from 0.19921875 to 1
- expert_gate: bfloat16 [16, 1024, 256], P('ep', None, 'tp'), may hold values from -0.1875 to 0.1875
- expert_up: bfloat16 [16, 1024, 256], P('ep', None, 'tp'), may hold values from -0.1875 to 0.1875
- expert_down: bfloat16 [16, 256, 1024], P('ep', 'tp'), may hold values from -0.375 to 0.375
- dense_gate: bfloat16 [1024, 4096], P('tp', 'ep'), may hold values from -0.1875 to 0.1875
- dense_up: bfloat16 [1024, 4096], P('tp', 'ep'), may hold values from -0.1875 to 0.1875
- dense_down: bfloat16 [4096, 1024], P('ep', 'tp'), may hold values from -0.1875 to 0.1875
- branch_gate: float32 [1024], replicated, may hold values from -0.1875 to 0.1875
Outputs:
- layer_out: bfloat16 [256, 1024], P('ep', 'tp')
Inputs may be any that keep to these rules, and one draw needn't show every extreme that they name: `expert_ids`: each row names 6 different experts; among the 16 rows of one index of ep no expert is named by more than 12 rows. `seq_lengths`: some sequence has all 1024 positions live.
All inputs are finite; a program needn't handle non-finite values.
Results may differ from a plain program's by a relative error of at most 0.017.
The roundings to bfloat16 on the way count: a program that leaves them out, or rounds other values in their place, can miss the bound.
Values may be sent and summed in bfloat16 or wider, within the bound.
A program may use at most 64 MiB of HBM per device.

v0:
```python
import jax
import jax.numpy as jnp
from jax import lax
from jax.sharding import PartitionSpec as P

HD = 64
NORM_EPS = 1e-06
HEAD_EPS = 1e-05
THETA = 500000.0
LAMBDA_BASE = 0.2


def norm_rows(values, gain_vec, epsilon):
    mean_square = jnp.mean(values * values, axis=-1, keepdims=True)
    return values * lax.rsqrt(mean_square + epsilon) * gain_vec


def rotate(values, position):
    half_dim = HD // 2
    frequency = THETA ** (-jnp.arange(half_dim, dtype=jnp.float32) * (2.0 / HD))
    angles = position.astype(jnp.float32)[:, None] * frequency[None, :]
    cos_vals = jnp.cos(angles)[:, None, :]
    sin_vals = jnp.sin(angles)[:, None, :]
    first_half = values[..., :half_dim]
    second = values[..., half_dim:]
    return jnp.concatenate(
        [first_half * cos_vals - second * sin_vals, second * cos_vals + first_half * sin_vals],
        axis=-1,
    )


def expert_rows(arrived, expert_gate, expert_up, expert_down):
    source_count, slot_count, model_width = arrived.shape
    stacked = arrived.reshape(source_count * slot_count, model_width)
    gate_part = jnp.dot(stacked, expert_gate[0], preferred_element_type=jnp.float32)
    up_part = jnp.dot(stacked, expert_up[0], preferred_element_type=jnp.float32)
    expert_hidden = (jax.nn.silu(gate_part) * up_part).astype(jnp.bfloat16)
    partial_value = jnp.dot(expert_hidden, expert_down[0], preferred_element_type=jnp.float32)
    partial_value = partial_value.reshape(source_count, slot_count, model_width)
    return lax.psum_scatter(
        partial_value.astype(jnp.bfloat16), "tp", scatter_dimension=2, tiled=True
    )


def dense_branch(partials, dense_down):
    summed = lax.psum(partials.astype(jnp.bfloat16), "tp").astype(jnp.float32)
    unit_count = partials.shape[1] // 2
    dense_hidden = (jax.nn.silu(summed[:, :unit_count]) * summed[:, unit_count:]).astype(
        jnp.bfloat16
    )
    return jnp.dot(dense_hidden, dense_down, preferred_element_type=jnp.float32)


def shards(
    tokens,
    mixer_gain,
    query_weight,
    key_weight,
    value_weight,
    head_lambda,
    head_gain,
    out_weight,
    cache_keys,
    cache_values,
    seq_lengths,
    channel_gain,
    expert_ids,
    expert_shares,
    expert_gate,
    expert_up,
    expert_down,
    dense_gate,
    dense_up,
    dense_down,
    branch_gate,
):
    seq_count, model_width = tokens.shape
    resid = tokens.astype(jnp.float32)
    normed = norm_rows(resid, mixer_gain, NORM_EPS).astype(jnp.bfloat16)
    value_width = 2 * HD
    groups = cache_values.shape[2] // value_width
    local_heads = head_lambda.shape[0]
    per_group = local_heads // groups
    cache_span = cache_keys.shape[1]
    query_raw = jnp.dot(normed, query_weight, preferred_element_type=jnp.float32).reshape(
        seq_count, local_heads * 2, HD
    )
    key_raw = jnp.dot(normed, key_weight, preferred_element_type=jnp.float32).reshape(
        seq_count, groups * 2, HD
    )
    value_new = jnp.dot(normed, value_weight, preferred_element_type=jnp.float32).astype(
        jnp.bfloat16
    )
    value_new = value_new.reshape(seq_count, groups, value_width)
    query = (
        rotate(query_raw, seq_lengths)
        .astype(jnp.bfloat16)
        .reshape(seq_count, groups, per_group, 2, HD)
    )
    key_new = rotate(key_raw, seq_lengths).astype(jnp.bfloat16).reshape(seq_count, groups, 2, HD)
    key_rows = cache_keys.reshape(seq_count, cache_span, groups, 2, HD)
    value_rows = cache_values.reshape(seq_count, cache_span, groups, value_width)
    lambdas = head_lambda.reshape(groups, per_group)
    score_scale = HD ** (-0.5)
    scores = (
        jnp.einsum("sgjcd,slgcd->sgjcl", query, key_rows, preferred_element_type=jnp.float32)
        * score_scale
    )
    fresh_score = (
        jnp.einsum("sgjcd,sgcd->sgjc", query, key_new, preferred_element_type=jnp.float32)
        * score_scale
    )
    live = jnp.arange(cache_span)[None, :] < seq_lengths[:, None]
    scores = jnp.where(live[:, None, None, None, :], scores, -jnp.inf)
    peak = jnp.maximum(jnp.max(scores, axis=-1), fresh_score)
    expo_scores = jnp.exp(scores - peak[..., None])
    expo_fresh = jnp.exp(fresh_score - peak)
    denom_sum = jnp.sum(expo_scores, axis=-1) + expo_fresh
    probability = expo_scores / denom_sum[..., None]
    prob_fresh = expo_fresh / denom_sum
    weight = (probability[:, :, :, 0] - lambdas[None, :, :, None] * probability[:, :, :, 1]).astype(
        jnp.bfloat16
    )
    weight_fresh = (prob_fresh[..., 0] - lambdas[None] * prob_fresh[..., 1]).astype(jnp.bfloat16)
    head_mix = jnp.einsum("sgjl,slgv->sgjv", weight, value_rows, preferred_element_type=jnp.float32)
    head_mix = (
        head_mix
        + weight_fresh.astype(jnp.float32)[..., None] * value_new.astype(jnp.float32)[:, :, None, :]
    )
    head_mix = head_mix.reshape(seq_count, local_heads, value_width)
    head_out = (norm_rows(head_mix, head_gain, HEAD_EPS) * (1.0 - LAMBDA_BASE)).astype(jnp.bfloat16)
    attn_part = jnp.dot(
        head_out.reshape(seq_count, local_heads * value_width),
        out_weight,
        preferred_element_type=jnp.float32,
    )
    attn_sum = lax.psum(attn_part.astype(jnp.bfloat16), "tp").astype(jnp.float32)
    resid_mid = (resid + attn_sum).astype(jnp.bfloat16)
    ffn_input = norm_rows(resid_mid.astype(jnp.float32), channel_gain, NORM_EPS).astype(
        jnp.bfloat16
    )
    gate_own = jax.nn.sigmoid(
        jnp.dot(ffn_input.astype(jnp.float32), branch_gate, precision=lax.Precision.HIGHEST)
    )
    half_width = model_width // lax.axis_size("tp")
    offset = lax.axis_index("tp") * half_width
    mid_half = lax.dynamic_slice_in_dim(resid_mid, offset, half_width, 1)
    experts_total = lax.axis_size("ep")
    top_count = expert_ids.shape[1]
    capacity = max(2, 2 * seq_count * top_count // experts_total)
    slot_ids = jnp.arange(1, capacity + 1, dtype=jnp.int32)
    named_mask = expert_ids[:, :, None] == jnp.arange(experts_total, dtype=jnp.int32)[None, None, :]
    picked = jnp.any(named_mask, axis=1)
    share_wide = expert_shares.astype(jnp.float32)[:, :, None]
    row_share = jnp.sum(jnp.where(named_mask, share_wide, jnp.zeros_like(share_wide)), axis=1)
    slot_rank = jnp.cumsum(picked.astype(jnp.int32), axis=0)
    placed = picked[None, :, :] & (slot_rank[None, :, :] == slot_ids[:, None, None])
    outgoing = jnp.einsum(
        "cse,sd->ecd", placed.astype(jnp.bfloat16), ffn_input, preferred_element_type=jnp.float32
    ).astype(jnp.bfloat16)
    expert_out = expert_rows(
        lax.all_to_all(outgoing, "ep", split_axis=0, concat_axis=0, tiled=True),
        expert_gate,
        expert_up,
        expert_down,
    )
    returned = lax.all_to_all(expert_out, "ep", split_axis=0, concat_axis=0, tiled=True)
    routed_sum = jnp.einsum(
        "cse,ecd->sd",
        placed.astype(jnp.float32) * row_share[None],
        returned.astype(jnp.float32),
        precision=lax.Precision.HIGHEST,
    )
    input_half = lax.dynamic_slice_in_dim(ffn_input, offset, half_width, 1)
    piece_rows = lax.all_gather(input_half, "ep", axis=0, tiled=True)
    partials = jnp.concatenate(
        [
            jnp.dot(piece_rows, dense_gate, preferred_element_type=jnp.float32),
            jnp.dot(piece_rows, dense_up, preferred_element_type=jnp.float32),
        ],
        axis=1,
    )
    branch_term = dense_branch(partials, dense_down)
    summed = lax.psum_scatter(branch_term, "ep", scatter_dimension=0, tiled=True)
    summed = gate_own[:, None] * summed + routed_sum
    return (mid_half.astype(jnp.float32) + summed).astype(jnp.bfloat16)


def solution(mesh):
    placed = (
        P("ep", None),
        P(),
        P(None, "tp"),
        P(None, "tp"),
        P(None, "tp"),
        P("tp"),
        P(),
        P("tp", None),
        P("ep", None, "tp"),
        P("ep", None, "tp"),
        P("ep"),
        P(),
        P("ep", None),
        P("ep", None),
        P("ep", None, "tp"),
        P("ep", None, "tp"),
        P("ep", "tp", None),
        P("tp", "ep"),
        P("tp", "ep"),
        P("ep", "tp"),
        P(),
    )
    return jax.shard_map(
        shards, mesh=mesh, in_specs=placed, out_specs=P("ep", "tp"), check_vma=False
    )
```

profile of v0, /device:TPU:0, one launch (start us, length us, event | category | flops | bytes accessed | tf_op | source)
XLA Modules:
  0.0 203.1 jit_solution(3398508565920873563)
XLA Ops:
  6.5 0.7 convert_element_type.100
  7.3 0.7 iota_compare_fusion
  8.0 0.9 fusion.32
  8.9 1.2 fusion.59
  10.2 1.6 fusion.61
  12.6 6.4 %copy.65 = bf16[16,1024,128]{1,2,0:T(8,128)(2,1)} copy(bf16[16,1024,128]{2,1,0:T(8,128)(2,1)} %param.29) | data formatting | bytes 8388608 | tf_op args[8]
  19.1 3.0 %fusion.65 = (f32[16,4,2]{1,2,0:T(2,128)S(1)}, f32[16,1,4,2,1024]{4,2,3,0,1:T(4,128)S(1)}) fusion(bf16[16,1024,2,64]{1,3,2,0:T(8,128)(2,1)} %bitcast.151, bf16[16,4,2,32]{3,1,2,0:T(4,128)(2,1)S(1)} %copy.64, bf16[16,4,2,32]{3,1,2,0:T(4,128)(2,1)S(1)} %copy.63, pred[16,1024]{1,0:T(8,128)(4,1)S(1)} %iota_compare_fusion), kind=kOutput, calls=%fused_computation.106 | convolution fusion | flops 17203072 | bytes 4751872 | tf_op jit(solution)/shard_map/sgjcd,slgcd->sgjcl/dot_general | solution.py:106
  22.3 0.3 fusion.13
  22.9 0.3 fusion.12
  23.6 3.0 %multiply_reduce_fusion = (f32[16,4]{1,0:T(8,128)S(1)}, f32[16,4,128]{2,1,0:T(4,128)S(1)}) fusion(f32[16,128]{1,0:T(8,128)S(1)} %fusion.7, f32[16,4]{1,0:T(8,128)S(1)} %copy.71, bf16[16,1024,128]{2,1,0:T(8,128)(2,1)} %param.30, f32[16,1,4,2,1024]{4,2,3,0,1:T(4,128)S(1)} %fusion.12, f32[4]{0:T(128)S(1)} %copy-done.9), kind=kOutput, calls=%fused_computation.69 | convolution fusion | flops 17006528 | bytes 4760080 | tf_op jit(solution)/shard_map/sgjl,slgv->sgjv/dot_general | solution.py:125
  27.0 3.7 %psum.14 = bf16[16,1024]{1,0:T(8,128)(2,1)S(1)} all-reduce(bf16[16,1024]{1,0:T(8,128)(2,1)S(1)} %convolution_convert_fusion.3), channel_id=1, replica_groups=mesh['ep'=16,'tp'=2] {'tp'}, use_global_device_ids=true, to_apply=%region_4.5 | all-reduce | flops 16384 | bytes 65536 | tf_op jit(solution)/shard_map/psum | solution.py:137
  31.6 1.0 copy.73
  32.6 8.2 %all-to-all-start = ((bf16[16,12,1024]{2,1,0:T(8,128)(2,1)}), bf16[16,12,1024]{2,1,0:T(8,128)(2,1)S(1)}, u32[]{:S(2)}, u32[]{:S(2)}) async-start(bf16[16,12,1024]{2,1,0:T(8,128)(2,1)} %copy.73), calls=%async_computation.1 | async-start | bytes 1048576 | tf_op jit(solution)/shard_map/all_to_all | solution.py:162
  40.9 44.5 %all_gather.3 = bf16[256,512]{1,0:T(8,128)(2,1)S(1)} all-gather(bf16[16,512]{1,0:T(8,128)(2,1)S(1)} %constant_dynamic-slice_fusion), channel_id=1, replica_groups=mesh['ep'=16,'tp'=2] {'ep'}, dimensions={0}, use_global_device_ids=true | all-gather | bytes 278528 | tf_op jit(solution)/shard_map/all_gather | solution.py:175
  85.9 0.7 pad_maximum_fusion
  87.4 1.0 convolution_convert_fusion
  88.5 13.9 %all-reduce.2.cloned.1.call-done = bf16[256,512]{0,1:T(8,128)(2,1)} async-done(((bf16[256,512]{0,1:T(8,128)(2,1)}), bf16[256,512]{0,1:T(8,128)(2,1)}) %all-reduce.2.cloned.1.call-update) | async-done | bytes 262160 | tf_op jit(solution)/shard_map/psum | solution.py:46
  102.3 1.0 convert_element_type.112
  103.3 1.1 fusion.24
  104.4 9.2 %reduce-scatter.5.cloned.1.call-done = bf16[16,12,512]{2,0,1:T(8,128)(2,1)} async-done(((bf16[16,12,1024]{2,0,1:T(8,128)(2,1)}), bf16[16,12,512]{2,0,1:T(8,128)(2,1)}) %reduce-scatter.5.cloned.1.call-update) | async-done | bytes 196624 | tf_op jit(solution)/shard_map/reduce_scatter | solution.py:40
  113.7 1.7 copy.75
  115.4 6.7 %all-to-all-start.1 = ((bf16[16,12,512]{2,1,0:T(8,128)(2,1)}), bf16[16,12,512]{2,1,0:T(8,128)(2,1)S(1)}, u32[]{:S(2)}, u32[]{:S(2)}) async-start(bf16[16,12,512]{2,1,0:T(8,128)(2,1)} %copy.75), calls=%async_computation.3 | async-start | bytes 524288 | tf_op jit(solution)/shard_map/all_to_all | solution.py:167
  122.4 72.4 %reduce-scatter.3.cloned.1.call-done = f32[16,512]{1,0:T(8,128)} async-done(((f32[256,512]{1,0:T(8,128)}), f32[16,512]{1,0:T(8,128)}) %reduce-scatter.3.cloned.1.call-update) | async-done | bytes 32784 | tf_op jit(solution)/shard_map/reduce_scatter | solution.py:184
  194.8 1.8 fusion.6
  (87 shorter events, 4.5 us)
Async XLA Ops:
  6.5 20.2 %copy-start = (bf16[512,1024]{1,0:T(8,128)(2,1)S(1)}, bf16[512,1024]{1,0:T(8,128)(2,1)}, u32[]{:S(2)}) copy-start(bf16[512,1024]{1,0:T(8,128)(2,1)} %param.28) | copy-start | bytes 3145732
  19.1 4.1 %copy-start.9 = (f32[4]{0:T(128)S(1)}, f32[4]{0:T(128)}, u32[]{:S(2)}) copy-start(f32[4]{0:T(128)} %param.26) | copy-start | bytes 52
  19.1 4.3 %copy-start.1 = (bf16[16,1024]{1,0:T(8,128)(2,1)S(1)}, bf16[16,1024]{1,0:T(8,128)(2,1)}, u32[]{:S(2)}) copy-start(bf16[16,1024]{1,0:T(8,128)(2,1)} %param.21) | copy-start | bytes 98308
  19.1 4.3 %copy-start.7 = (f32[1024]{0:T(1024)S(1)}, f32[1024]{0:T(1024)}, u32[]{:S(2)}) copy-start(f32[1024]{0:T(1024)} %param.22) | copy-start | bytes 12292
  19.1 4.3 %copy-start.12 = (bf16[1024,128]{1,0:T(8,128)(2,1)S(1)}, bf16[1024,128]{1,0:T(8,128)(2,1)}, u32[]{:S(2)}) copy-start(bf16[1024,128]{1,0:T(8,128)(2,1)} %param.25) | copy-start | bytes 786436
  22.1 4.5 %copy-start.11 = (f32[128]{0:T(128)S(1)}, f32[128]{0:T(128)}, u32[]{:S(2)}) copy-start(f32[128]{0:T(128)} %param.27) | copy-start | bytes 1540
  22.1 8.8 %copy-start.6 = (s32[16,6]{0,1:T(8,128)S(1)}, s32[16,6]{0,1:T(8,128)}, u32[]{:S(2)}) copy-start(s32[16,6]{0,1:T(8,128)} %param.33) | copy-start | bytes 1156
  22.1 9.1 %copy-start.8 = (f32[1024]{0:T(1024)S(1)}, f32[1024]{0:T(1024)}, u32[]{:S(2)}) copy-start(f32[1024]{0:T(1024)} %param.32) | copy-start | bytes 12292
  23.6 61.8 %copy-start.3 = (bf16[512,256]{1,0:T(8,128)(2,1)S(1)}, bf16[512,256]{1,0:T(8,128)(2,1)}, u32[]{:S(2)}) copy-start(bf16[512,256]{1,0:T(8,128)(2,1)} %param.39) | copy-start | bytes 786436
  26.6 59.0 %copy-start.4 = (bf16[512,256]{1,0:T(8,128)(2,1)S(1)}, bf16[512,256]{1,0:T(8,128)(2,1)}, u32[]{:S(2)}) copy-start(bf16[512,256]{1,0:T(8,128)(2,1)} %param.38) | copy-start | bytes 786436
  26.7 60.1 %copy-start.2 = (bf16[1,1024,128]{2,1,0:T(8,128)(2,1)S(1)}, bf16[1,1024,128]{2,1,0:T(8,128)(2,1)}, u32[]{:S(2)}) copy-start(bf16[1,1024,128]{2,1,0:T(8,128)(2,1)} %param.35) | copy-start | bytes 786436
  30.7 56.4 %copy-start.13 = (bf16[1,1024,128]{2,1,0:T(8,128)(2,1)S(1)}, bf16[1,1024,128]{2,1,0:T(8,128)(2,1)}, u32[]{:S(2)}) copy-start(bf16[1,1024,128]{2,1,0:T(8,128)(2,1)} %param.36) | copy-start | bytes 786436
  31.6 55.8 %copy-start.5 = (bf16[1,128,1024]{2,1,0:T(8,128)(2,1)S(1)}, bf16[1,128,1024]{2,1,0:T(8,128)(2,1)}, u32[]{:S(2)}) copy-start(bf16[1,128,1024]{2,1,0:T(8,128)(2,1)} %param.37) | copy-start | bytes 786436
  32.6 70.7 %copy-start.14 = (bf16[256,512]{1,0:T(8,128)(2,1)S(1)}, bf16[256,512]{1,0:T(8,128)(2,1)}, u32[]{:S(2)}) copy-start(bf16[256,512]{1,0:T(8,128)(2,1)} %param.40) | copy-start | bytes 786436
  32.6 54.1 %all-to-all-start = ((bf16[16,12,1024]{2,1,0:T(8,128)(2,1)}), bf16[16,12,1024]{2,1,0:T(8,128)(2,1)S(1)}, u32[]{:S(2)}, u32[]{:S(2)}) async-start(bf16[16,12,1024]{2,1,0:T(8,128)(2,1)} %copy.73), calls=%async_computation.1 | async-start | bytes 1048576 | tf_op jit(solution)/shard_map/all_to_all | solution.py:162
  40.8 61.5 %all-reduce.2.cloned.1.call-start = ((), (), s32[]{:S(2)}) async-start(), calls=%async_computation.4 | async-start | bytes 524288 | tf_op jit(solution)/shard_map/psum | solution.py:46
  85.9 36.2 %copy-start.10 = (bf16[16,6]{0,1:T(8,128)(2,1)S(1)}, bf16[16,6]{0,1:T(8,128)(2,1)}, u32[]{:S(2)}) copy-start(bf16[16,6]{0,1:T(8,128)(2,1)} %param.34) | copy-start | bytes 580
  86.6 35.6 %copy-start.15 = (f32[1024]{0:T(1024)S(1)}, f32[1024]{0:T(1024)}, u32[]{:S(2)}) copy-start(f32[1024]{0:T(1024)} %param.41) | copy-start | bytes 12292
  86.7 27.0 %reduce-scatter.5.cloned.1.call-start = ((), (), s32[]{:S(2)}) async-start(), calls=%async_computation.6 | async-start | bytes 589824 | tf_op jit(solution)/shard_map/reduce_scatter | solution.py:40
  88.4 106.4 %reduce-scatter.3.cloned.1.call-start = ((), (), s32[]{:S(2)}) async-start(), calls=%async_computation.5 | async-start | bytes 557056 | tf_op jit(solution)/shard_map/reduce_scatter | solution.py:184
  115.4 79.4 %all-to-all-start.1 = ((bf16[16,12,512]{2,1,0:T(8,128)(2,1)}), bf16[16,12,512]{2,1,0:T(8,128)(2,1)S(1)}, u32[]{:S(2)}, u32[]{:S(2)}) async-start(bf16[16,12,512]{2,1,0:T(8,128)(2,1)} %copy.75), calls=%async_computation.3 | async-start | bytes 524288 | tf_op jit(solution)/shard_map/all_to_all | solution.py:167
Sparse Core Ops, SparseCore 0:
  86.8 15.5 all-reduce.1
  104.6 9.0 reduce-scatter.4
  115.9 78.8 reduce-scatter.2
where the time goes:
time: 204 us; the launch traced here: 203 us
  waiting for transfers between devices  95.6 us (47%)
  blocking collectives  48.2 us (24%)
  starting transfers between devices  15 us (7%)
  matrix products  14.8 us (7%)
  between operations  13.5 us (7%)
  local copies, waits for them, and re-layouts  10.3 us (5%)
  other arithmetic  5.81 us (3%)
    reduce_scatter x1, waiting for transfers between devices, shards(): lax.psum_scatter(branch_term, 'ep', scatter_dimension=0, tiled=True)  72.4 us
    all_gather x1, blocking collectives, shards(): piece_rows = lax.all_gather(input_half, 'ep', axis=0, tiled=True)  44.5 us
    psum x1, waiting for transfers between devices, dense_branch(): summed = lax.psum(partials.astype(jnp.bfloat16), 'tp').astype(jnp.float32)  13.9 us
    reduce_scatter x1, waiting for transfers between devices, expert_rows(): lax.psum_scatter(partial_value.astype(jnp.bfloat16), 'tp', scatter_dimens...  9.22 us
    all_to_all x1, starting transfers between devices, shards(): lax.all_to_all(outgoing, 'ep', split_axis=0, concat_axis=0, tiled=True)  8.15 us
    all_to_all x1, starting transfers between devices, shards(): lax.all_to_all(expert_out, 'ep', split_axis=0, concat_axis=0, tiled=True)  6.71 us
    unnamed x33, local copies, waits for them, and re-layouts  6.48 us
  transfers between devices with their start and end apart: 5, of which 3 were waited for; matrix products, arithmetic and copies ran while one was open for 3% of the time, Pallas kernels for 0%

commit v1 on v0

--- a/solution.py
+++ b/solution.py
@@ -8,6 +8,12 @@
 HEAD_EPS = 1e-05
 THETA = 500000.0
 LAMBDA_BASE = 0.2
+
+
+def add_all(array, name):
+    parts = lax.all_gather(array, name, axis=0, tiled=False)
+    total = parts.sum(axis=0)
+    return total
 
 
 def norm_rows(values, gain_vec, epsilon):
@@ -43,7 +49,7 @@
 
 
 def dense_branch(partials, dense_down):
-    summed = lax.psum(partials.astype(jnp.bfloat16), "tp").astype(jnp.float32)
+    summed = add_all(partials.astype(jnp.bfloat16), "tp").astype(jnp.float32)
     unit_count = partials.shape[1] // 2
     dense_hidden = (jax.nn.silu(summed[:, :unit_count]) * summed[:, unit_count:]).astype(
         jnp.bfloat16

time: 204 us -> 185 us (0.907)
  waiting for transfers between devices: 95.6 us -> 83.6 us
  starting transfers between devices: 15 us -> 11.6 us
  blocking collectives: 48.2 us -> 45.4 us
    all_to_all x1, waiting for transfers between devices: 0.01 us -> 15.4 us  [shards(): lax.all_to_all(outgoing, 'ep', split_axis=0, concat_axis=0, tiled=True)]
    psum x1 -> x0, waiting for transfers between devices: 13.9 us -> none  [dense_branch(): summed = lax.psum(partials.astype(jnp.bfloat16), 'tp').astype(jnp.float32)]
    reduce_scatter x1, waiting for transfers between devices: 9.22 us -> 0.02 us  [expert_rows(): lax.psum_scatter(partial_value.astype(jnp.bfloat16), 'tp', scatter_dimens...]
    all_gather x1, blocking collectives: 44.5 us -> 39.5 us  [shards(): piece_rows = lax.all_gather(input_half, 'ep', axis=0, tiled=True)]
    reduce_scatter x1, waiting for transfers between devices: 72.4 us -> 68.2 us  [shards(): lax.psum_scatter(branch_term, 'ep', scatter_dimension=0, tiled=True)]
    all_to_all x1, starting transfers between devices: 6.71 us -> 3.53 us  [shards(): lax.all_to_all(expert_out, 'ep', split_axis=0, concat_axis=0, tiled=True)]
    all_gather x0 -> x1, blocking collectives: none -> 2.18 us  [add_all(): parts = lax.all_gather(array, name, axis=0, tiled=False)]
    unnamed x33 -> x34, local copies, waits for them, and re-layouts: 6.48 us -> 6.62 us
  transfers between devices with their start and end apart: 5 -> 4, of which waited for: 3 -> 2; matrix products, arithmetic and copies ran while one was open for 3% -> 2% of each run, Pallas kernels for 0% -> 0%
where the time goes in v1:
time: 185 us; the launch traced here: 184 us
  waiting for transfers between devices  83.6 us (45%)
  blocking collectives  45.4 us (25%)
  matrix products  14.8 us (8%)
  between operations  13.8 us (7%)
  starting transfers between devices  11.6 us (6%)
  local copies, waits for them, and re-layouts  10.6 us (6%)
  other arithmetic  4.25 us (2%)
    reduce_scatter x1, waiting for transfers between devices, shards(): lax.psum_scatter(branch_term, 'ep', scatter_dimension=0, tiled=True)  68.2 us
    all_gather x1, blocking collectives, shards(): piece_rows = lax.all_gather(input_half, 'ep', axis=0, tiled=True)  39.5 us
    all_to_all x1, waiting for transfers between devices, shards(): lax.all_to_all(outgoing, 'ep', split_axis=0, concat_axis=0, tiled=True)  15.4 us
    all_to_all x1, starting transfers between devices, shards(): lax.all_to_all(outgoing, 'ep', split_axis=0, concat_axis=0, tiled=True)  8.02 us
    unnamed x34, local copies, waits for them, and re-layouts  6.62 us
    psum x1, blocking collectives, shards(): lax.psum(attn_part.astype(jnp.bfloat16), 'tp').astype(jnp.float32)  3.72 us
  transfers between devices with their start and end apart: 4, of which 2 were waited for; matrix products, arithmetic and copies ran while one was open for 2% of the time, Pallas kernels for 0%

profile of v1, /device:TPU:0, one launch (start us, length us, event | category | flops | bytes accessed | tf_op | source)
XLA Modules:
  0.0 184.1 jit_solution(3862367035761697274)
XLA Ops:
  6.5 0.7 convert_element_type.109
  7.3 0.7 iota_compare_fusion
  8.0 0.9 fusion.34
  8.9 1.2 fusion.61
  10.2 1.6 fusion.63
  12.6 6.4 %copy.67 = bf16[16,1024,128]{1,2,0:T(8,128)(2,1)} copy(bf16[16,1024,128]{2,1,0:T(8,128)(2,1)} %param.29) | data formatting | bytes 8388608 | tf_op args[8]
  19.1 3.0 %fusion.67 = (f32[16,4,2]{1,2,0:T(2,128)S(1)}, f32[16,1,4,2,1024]{4,2,3,0,1:T(4,128)S(1)}) fusion(bf16[16,1024,2,64]{1,3,2,0:T(8,128)(2,1)} %bitcast.155, bf16[16,4,2,32]{3,1,2,0:T(4,128)(2,1)S(1)} %copy.66, bf16[16,4,2,32]{3,1,2,0:T(4,128)(2,1)S(1)} %copy.65, pred[16,1024]{1,0:T(8,128)(4,1)S(1)} %iota_compare_fusion), kind=kOutput, calls=%fused_computation.108 | convolution fusion | flops 17203072 | bytes 4751872 | tf_op jit(solution)/shard_map/sgjcd,slgcd->sgjcl/dot_general | solution.py:112
  22.3 0.3 fusion.15
  22.9 0.3 fusion.14
  23.6 3.0 %multiply_reduce_fusion = (f32[16,4]{1,0:T(8,128)S(1)}, f32[16,4,128]{2,1,0:T(4,128)S(1)}) fusion(f32[16,128]{1,0:T(8,128)S(1)} %fusion.9, f32[16,4]{1,0:T(8,128)S(1)} %copy.73, bf16[16,1024,128]{2,1,0:T(8,128)(2,1)} %param.30, f32[16,1,4,2,1024]{4,2,3,0,1:T(4,128)S(1)} %fusion.14, f32[4]{0:T(128)S(1)} %copy-done.9), kind=kOutput, calls=%fused_computation.71 | convolution fusion | flops 17006528 | bytes 4760080 | tf_op jit(solution)/shard_map/sgjl,slgv->sgjv/dot_general | solution.py:131
  27.0 3.7 %psum.7 = bf16[16,1024]{1,0:T(8,128)(2,1)S(1)} all-reduce(bf16[16,1024]{1,0:T(8,128)(2,1)S(1)} %convolution_convert_fusion.3), channel_id=1, replica_groups=mesh['ep'=16,'tp'=2] {'tp'}, use_global_device_ids=true, to_apply=%region_4.5 | all-reduce | flops 16384 | bytes 65536 | tf_op jit(solution)/shard_map/psum | solution.py:143
  31.6 1.0 copy.77
  32.6 8.0 %all-to-all-start = ((bf16[16,12,1024]{2,1,0:T(8,128)(2,1)}), bf16[16,12,1024]{2,1,0:T(8,128)(2,1)S(1)}, u32[]{:S(2)}, u32[]{:S(2)}) async-start(bf16[16,12,1024]{2,1,0:T(8,128)(2,1)} %copy.77), calls=%async_computation.1 | async-start | bytes 1048576 | tf_op jit(solution)/shard_map/all_to_all | solution.py:168
  40.7 15.4 %all-to-all-done = bf16[16,12,1024]{2,1,0:T(8,128)(2,1)S(1)} async-done(((bf16[16,12,1024]{2,1,0:T(8,128)(2,1)}), bf16[16,12,1024]{2,1,0:T(8,128)(2,1)S(1)}, u32[]{:S(2)}, u32[]{:S(2)}) %all-to-all-start) | async-done | bytes 393248 | tf_op jit(solution)/shard_map/all_to_all | solution.py:168
  56.8 1.0 convolution_convert_fusion
  57.9 39.5 %all_gather.7 = bf16[256,512]{1,0:T(8,128)(2,1)S(1)} all-gather(bf16[16,512]{1,0:T(8,128)(2,1)S(1)} %constant_dynamic-slice_fusion), channel_id=1, replica_groups=mesh['ep'=16,'tp'=2] {'ep'}, dimensions={0}, use_global_device_ids=true | all-gather | bytes 278528 | tf_op jit(solution)/shard_map/all_gather | solution.py:181
  97.4 0.3 fusion.3
  97.7 0.3 fusion.4
  98.1 2.2 %all_gather.8 = bf16[2,256,512]{2,1,0:T(8,128)(2,1)S(1)} all-gather(bf16[1,256,512]{2,1,0:T(8,128)(2,1)S(1)} %copy.74), channel_id=1, replica_groups=mesh['ep'=16,'tp'=2] {'tp'}, dimensions={0}, use_global_device_ids=true | all-gather | bytes 786432 | tf_op jit(solution)/shard_map/all_gather | solution.py:14
  100.6 1.1 fusion.26
  101.7 1.7 copy.79
  103.5 3.5 %all-to-all-start.1 = ((bf16[16,12,512]{2,1,0:T(8,128)(2,1)}), bf16[16,12,512]{2,1,0:T(8,128)(2,1)S(1)}, u32[]{:S(2)}, u32[]{:S(2)}) async-start(bf16[16,12,512]{2,1,0:T(8,128)(2,1)} %copy.79), calls=%async_computation.3 | async-start | bytes 524288 | tf_op jit(solution)/shard_map/all_to_all | solution.py:173
  107.3 68.2 %reduce-scatter.3.cloned.1.call-done = f32[16,512]{1,0:T(8,128)} async-done(((f32[256,512]{1,0:T(8,128)}), f32[16,512]{1,0:T(8,128)}) %reduce-scatter.3.cloned.1.call-update) | async-done | bytes 32784 | tf_op jit(solution)/shard_map/reduce_scatter | solution.py:190
  175.4 1.8 fusion.8
  (88 shorter events, 4.3 us)
Async XLA Ops:
  6.5 20.2 %copy-start = (bf16[512,1024]{1,0:T(8,128)(2,1)S(1)}, bf16[512,1024]{1,0:T(8,128)(2,1)}, u32[]{:S(2)}) copy-start(bf16[512,1024]{1,0:T(8,128)(2,1)} %param.28) | copy-start | bytes 3145732
  19.1 4.1 %copy-start.9 = (f32[4]{0:T(128)S(1)}, f32[4]{0:T(128)}, u32[]{:S(2)}) copy-start(f32[4]{0:T(128)} %param.26) | copy-start | bytes 52
  19.1 4.3 %copy-start.1 = (bf16[16,1024]{1,0:T(8,128)(2,1)S(1)}, bf16[16,1024]{1,0:T(8,128)(2,1)}, u32[]{:S(2)}) copy-start(bf16[16,1024]{1,0:T(8,128)(2,1)} %param.21) | copy-start | bytes 98308
  19.1 4.3 %copy-start.7 = (f32[1024]{0:T(1024)S(1)}, f32[1024]{0:T(1024)}, u32[]{:S(2)}) copy-start(f32[1024]{0:T(1024)} %param.22) | copy-start | bytes 12292
  19.1 4.3 %copy-start.12 = (bf16[1024,128]{1,0:T(8,128)(2,1)S(1)}, bf16[1024,128]{1,0:T(8,128)(2,1)}, u32[]{:S(2)}) copy-start(bf16[1024,128]{1,0:T(8,128)(2,1)} %param.25) | copy-start | bytes 786436
  22.1 4.5 %copy-start.11 = (f32[128]{0:T(128)S(1)}, f32[128]{0:T(128)}, u32[]{:S(2)}) copy-start(f32[128]{0:T(128)} %param.27) | copy-start | bytes 1540
  22.1 8.7 %copy-start.6 = (s32[16,6]{0,1:T(8,128)S(1)}, s32[16,6]{0,1:T(8,128)}, u32[]{:S(2)}) copy-start(s32[16,6]{0,1:T(8,128)} %param.33) | copy-start | bytes 1156
  22.1 9.0 %copy-start.8 = (f32[1024]{0:T(1024)S(1)}, f32[1024]{0:T(1024)}, u32[]{:S(2)}) copy-start(f32[1024]{0:T(1024)} %param.32) | copy-start | bytes 12292
  26.6 29.7 %copy-start.2 = (bf16[1,1024,128]{2,1,0:T(8,128)(2,1)S(1)}, bf16[1,1024,128]{2,1,0:T(8,128)(2,1)}, u32[]{:S(2)}) copy-start(bf16[1,1024,128]{2,1,0:T(8,128)(2,1)} %param.35) | copy-start | bytes 786436
  26.6 29.9 %copy-start.13 = (bf16[1,1024,128]{2,1,0:T(8,128)(2,1)S(1)}, bf16[1,1024,128]{2,1,0:T(8,128)(2,1)}, u32[]{:S(2)}) copy-start(bf16[1,1024,128]{2,1,0:T(8,128)(2,1)} %param.36) | copy-start | bytes 786436
  26.6 30.2 %copy-start.5 = (bf16[1,128,1024]{2,1,0:T(8,128)(2,1)S(1)}, bf16[1,128,1024]{2,1,0:T(8,128)(2,1)}, u32[]{:S(2)}) copy-start(bf16[1,128,1024]{2,1,0:T(8,128)(2,1)} %param.37) | copy-start | bytes 786436
  31.0 66.4 %copy-start.3 = (bf16[512,256]{1,0:T(8,128)(2,1)S(1)}, bf16[512,256]{1,0:T(8,128)(2,1)}, u32[]{:S(2)}) copy-start(bf16[512,256]{1,0:T(8,128)(2,1)} %param.38) | copy-start | bytes 786436
  31.5 66.2 %copy-start.4 = (bf16[512,256]{1,0:T(8,128)(2,1)S(1)}, bf16[512,256]{1,0:T(8,128)(2,1)}, u32[]{:S(2)}) copy-start(bf16[512,256]{1,0:T(8,128)(2,1)} %param.39) | copy-start | bytes 786436
  32.6 23.5 %all-to-all-start = ((bf16[16,12,1024]{2,1,0:T(8,128)(2,1)}), bf16[16,12,1024]{2,1,0:T(8,128)(2,1)S(1)}, u32[]{:S(2)}, u32[]{:S(2)}) async-start(bf16[16,12,1024]{2,1,0:T(8,128)(2,1)} %copy.77), calls=%async_computation.1 | async-start | bytes 1048576 | tf_op jit(solution)/shard_map/all_to_all | solution.py:168
  40.6 61.1 %reduce-scatter.5.cloned.1.call-start = ((), (), s32[]{:S(2)}) async-start(), calls=%async_computation.5 | async-start | bytes 589824 | tf_op jit(solution)/shard_map/reduce_scatter | solution.py:46
  56.2 44.4 %copy-start.14 = (bf16[256,512]{1,0:T(8,128)(2,1)S(1)}, bf16[256,512]{1,0:T(8,128)(2,1)}, u32[]{:S(2)}) copy-start(bf16[256,512]{1,0:T(8,128)(2,1)} %param.40) | copy-start | bytes 786436
  57.8 117.6 %reduce-scatter.3.cloned.1.call-start = ((), (), s32[]{:S(2)}) async-start(), calls=%async_computation.4 | async-start | bytes 557056 | tf_op jit(solution)/shard_map/reduce_scatter | solution.py:190
  97.4 9.6 %copy-start.10 = (bf16[16,6]{0,1:T(8,128)(2,1)S(1)}, bf16[16,6]{0,1:T(8,128)(2,1)}, u32[]{:S(2)}) copy-start(bf16[16,6]{0,1:T(8,128)(2,1)} %param.34) | copy-start | bytes 580
  97.4 9.8 %copy-start.15 = (f32[1024]{0:T(1024)S(1)}, f32[1024]{0:T(1024)}, u32[]{:S(2)}) copy-start(f32[1024]{0:T(1024)} %param.41) | copy-start | bytes 12292
  103.5 71.9 %all-to-all-start.1 = ((bf16[16,12,512]{2,1,0:T(8,128)(2,1)}), bf16[16,12,512]{2,1,0:T(8,128)(2,1)S(1)}, u32[]{:S(2)}, u32[]{:S(2)}) async-start(bf16[16,12,512]{2,1,0:T(8,128)(2,1)} %copy.79), calls=%async_computation.3 | async-start | bytes 524288 | tf_op jit(solution)/shard_map/all_to_all | solution.py:173
Sparse Core Ops, SparseCore 0:
  57.9 6.2 reduce-scatter.4
  101.8 73.5 reduce-scatter.2
